TPU v7x, 32 devices: a whole 2x2x4 slice. The times are simulated.
32 devices in a mesh: ep: 16 (over z, y, x), tp: 2 (over core).
Axes of the slice: x: 2, y: 2, z: 4, core: 2. Of those that a mesh axis runs over, the one named last changes fastest.
Arguments:
- tokens: bfloat16 [256, 2048], P('ep'), may hold values from -6 to 6
- norm_attn: float32 [2048], replicated, may hold values from 0.1 to 1.9
- w_query: bfloat16 [2048, 2048], P(None, 'tp'), may hold values from -0.125 to 0.125
- w_key: bfloat16 [2048, 256], P(None, 'tp'), may hold values from -0.125 to 0.125
- w_value: bfloat16 [2048, 256], P(None, 'tp'), may hold values from -0.125 to 0.125
- w_out: bfloat16 [2048, 2048], P('tp'), may hold values from -0.125 to 0.125
- attn_bias: float32 [32], P('tp'), may hold values from -7 to -1
- cache_keys: bfloat16 [256, 1024, 256], P('ep', None, 'tp'), may hold values from -6 to 6
- cache_values: bfloat16 [256, 1024, 256], P('ep', None, 'tp'), may hold values from -6 to 6
- lengths: int32 [256], P('ep'), may hold values from 256 to 1024
- norm_ffn: float32 [2048], replicated, may hold values from 0.1 to 1.9
- expert_gate: bfloat16 [2048, 57344], P(None, ('ep', 'tp')), may hold values from -0.125 to 0.125
- expert_up: bfloat16 [2048, 57344], P(None, ('ep', 'tp')), may hold values from -0.125 to 0.125
- expert_down: bfloat16 [57344, 2048], P(('ep', 'tp')), may hold values from -0.0625 to 0.0625
- dense_gate_w: bfloat16 [2048, 7168], P(None, 'ep'), may hold values from -0.125 to 0.125
- dense_up_w: bfloat16 [2048, 7168], P(None, 'ep'), may hold values from -0.125 to 0.125
- dense_down_w: bfloat16 [7168, 2048], P('ep'), may hold values from -0.0625 to 0.0625
- dense_mix: bfloat16 [2048], replicated, may hold values from -0.125 to 0.125
- routes: int32 [256, 2], P(('ep', 'tp')), may hold values from 0 to 7, all different within a row; in each aligned block of 8 rows (0 to 7, 8 to 15, ...) at most 3 rows name the same one
- route_weights: bfloat16 [256, 2], P(('ep', 'tp')), may hold values from 0.19921875 to 1
Outputs:
- layer_out: bfloat16 [256, 2048], P(('ep', 'tp'))
- new_keys: bfloat16 [256, 256], P('ep', 'tp')
- new_values: bfloat16 [256, 256], P('ep', 'tp')
Inputs may be any that keep to these rules, and one draw needn't show every extreme that they name: `routes`: in each aligned block of 8 rows (the rows of one device) no expert is named by more than 3 rows, a bound that some block reaches; a row names 2 different experts.
All inputs are finite; a program needn't handle non-finite values.
Results may differ from a plain program's by a relative error of at most 0.015.
Values may be sent and summed in bfloat16 or wider, within the bound.
A program may use at most 128 MiB of HBM per device.

v0:
```python
import jax
import jax.numpy as jnp
from jax import lax
from jax.sharding import PartitionSpec as P

HEAD_DIM = 64
EXPERTS = 8
TOP = 2
EPSILON = 1e-06


def normed_rows(values, gain):
    widened = values.astype(jnp.float32)
    scale = lax.rsqrt(jnp.mean(widened * widened, axis=-1, keepdims=True) + EPSILON)
    return (widened * scale * gain).astype(jnp.bfloat16)


def later_sums(log_keep):
    cache_len = log_keep.shape[-1]
    block_len = 128
    block_count = cache_len // block_len
    lead = log_keep.shape[:-1]
    blocked = log_keep.reshape(lead + (block_count, block_len))
    rows_in = lax.broadcasted_iota(jnp.int32, (block_len, block_len), 0)
    cols_in = lax.broadcasted_iota(jnp.int32, (block_len, block_len), 1)
    upper = (rows_in >= cols_in).astype(jnp.float32)
    within = jnp.einsum("...nj,ji->...ni", blocked, upper, precision=lax.Precision.HIGHEST)
    totals = within[..., 0]
    rows_out = lax.broadcasted_iota(jnp.int32, (block_count, block_count), 0)
    cols_out = lax.broadcasted_iota(jnp.int32, (block_count, block_count), 1)
    beyond = (rows_out > cols_out).astype(jnp.float32)
    following = jnp.einsum("...m,mn->...n", totals, beyond, precision=lax.Precision.HIGHEST)
    inclusive = within + following[..., None]
    return (inclusive - blocked).reshape(log_keep.shape)


def running_ranks(present):
    count = present.shape[-1]
    rows_in = lax.broadcasted_iota(jnp.int32, (count, count), 0)
    cols_in = lax.broadcasted_iota(jnp.int32, (count, count), 1)
    lower = (rows_in <= cols_in).astype(jnp.float32)
    totals = jnp.einsum(
        "...j,ji->...i", present.astype(jnp.float32), lower, precision=lax.Precision.HIGHEST
    )
    return totals.astype(jnp.int32) - 1


def shards(
    tokens,
    norm_attn,
    w_query,
    w_key,
    w_value,
    w_out,
    attn_bias,
    cache_keys,
    cache_values,
    lengths,
    norm_ffn,
    expert_gate,
    expert_up,
    expert_down,
    dense_gate_w,
    dense_up_w,
    dense_down_w,
    dense_mix,
    routes,
    route_weights,
):
    seq_count = tokens.shape[0]
    cache_len = cache_keys.shape[1]
    group_count = cache_keys.shape[2] // HEAD_DIM
    repeat = w_query.shape[1] // (group_count * HEAD_DIM)
    normed = normed_rows(tokens, norm_attn)
    query = jnp.dot(normed, w_query, preferred_element_type=jnp.float32).astype(jnp.bfloat16)
    new_keys = jnp.dot(normed, w_key, preferred_element_type=jnp.float32).astype(jnp.bfloat16)
    new_values = jnp.dot(normed, w_value, preferred_element_type=jnp.float32).astype(jnp.bfloat16)
    query_heads = query.reshape(seq_count, group_count, repeat, HEAD_DIM)
    key_heads = cache_keys.reshape(seq_count, cache_len, group_count, HEAD_DIM)
    value_heads = cache_values.reshape(seq_count, cache_len, group_count, HEAD_DIM)
    scores = jnp.einsum(
        "bgrd,bsgd->bgrs", query_heads, key_heads, preferred_element_type=jnp.float32
    ) * HEAD_DIM ** (-0.5)
    scores = scores + attn_bias.reshape(group_count, repeat)[None, :, :, None]
    places = lax.broadcasted_iota(jnp.int32, (seq_count, cache_len), 1)
    visible = (places < lengths[:, None])[:, None, None, :]
    log_keep = jnp.where(visible, jax.nn.log_sigmoid(-scores), 0.0)
    after = later_sums(log_keep)
    weight = jnp.where(visible, jnp.exp(jax.nn.log_sigmoid(scores) + after), 0.0).astype(
        jnp.bfloat16
    )
    heads_out = jnp.einsum(
        "bgrs,bsgd->bgrd", weight, value_heads, preferred_element_type=jnp.float32
    )
    heads_out = heads_out.astype(jnp.bfloat16).reshape(seq_count, group_count * repeat * HEAD_DIM)
    partial_value = jnp.dot(heads_out, w_out, preferred_element_type=jnp.float32)
    attn_sum = lax.psum_scatter(
        partial_value.astype(jnp.bfloat16), "tp", scatter_dimension=0, tiled=True
    ).astype(jnp.float32)
    row_count = seq_count // lax.axis_size("tp")
    capacity = (row_count * TOP + EXPERTS - 1) // EXPERTS + 1
    own_rows = lax.dynamic_slice_in_dim(tokens, lax.axis_index("tp") * row_count, row_count, 0)
    middle = (own_rows.astype(jnp.float32) + attn_sum).astype(jnp.bfloat16)
    normed_two = normed_rows(middle, norm_ffn)
    width = normed_two.shape[1]
    piece = lax.all_gather(normed_two, "ep", axis=0, tiled=True)
    mix_gate = jax.nn.sigmoid(jnp.dot(piece, dense_mix, preferred_element_type=jnp.float32))
    dense_hidden = (
        jax.nn.silu(jnp.dot(piece, dense_gate_w, preferred_element_type=jnp.float32))
        * jnp.dot(piece, dense_up_w, preferred_element_type=jnp.float32)
    ).astype(jnp.bfloat16)
    dense_terms = (
        jnp.dot(dense_hidden, dense_down_w, preferred_element_type=jnp.float32) * mix_gate[:, None]
    )
    dense_term = lax.psum_scatter(dense_terms, "ep", scatter_dimension=0, tiled=True)
    devices = lax.axis_size(("ep", "tp"))
    members = devices // EXPERTS
    expert_ids = lax.broadcasted_iota(jnp.int32, (EXPERTS, 1, 1), 0)
    matched = routes[None, :, :] == expert_ids
    present = jnp.any(matched, axis=2).astype(jnp.int32)
    share = jnp.sum(jnp.where(matched, route_weights.astype(jnp.float32)[None, :, :], 0.0), axis=2)
    ranks = running_ranks(present)
    slot_ids = lax.broadcasted_iota(jnp.int32, (EXPERTS, capacity, row_count), 1)
    selector = (present[:, None, :] == 1) & (ranks[:, None, :] == slot_ids)
    slot_rows = jnp.einsum(
        "ecr,rk->eck", selector.astype(jnp.bfloat16), normed_two, preferred_element_type=jnp.float32
    ).astype(jnp.bfloat16)
    outgoing = jnp.repeat(slot_rows, members, axis=0)
    incoming = lax.all_to_all(outgoing, ("ep", "tp"), split_axis=0, concat_axis=0, tiled=True)
    slot_rows = incoming.reshape(devices * capacity, width)
    expert_hidden = (
        jax.nn.silu(jnp.dot(slot_rows, expert_gate, preferred_element_type=jnp.float32))
        * jnp.dot(slot_rows, expert_up, preferred_element_type=jnp.float32)
    ).astype(jnp.bfloat16)
    expert_result = jnp.dot(expert_hidden, expert_down, preferred_element_type=jnp.float32).reshape(
        devices, capacity, width
    )
    back = lax.all_to_all(
        expert_result.astype(jnp.bfloat16), ("ep", "tp"), split_axis=0, concat_axis=0, tiled=True
    ).astype(expert_result.dtype)
    per_expert = jnp.sum(back.reshape(EXPERTS, members, capacity, width), axis=1)
    expert_term = jnp.einsum("ecr,eck,er->rk", selector.astype(jnp.float32), per_expert, share)
    layer_out = (middle.astype(jnp.float32) + expert_term + dense_term).astype(jnp.bfloat16)
    return (layer_out, new_keys, new_values)


def solution(mesh):
    placed = (
        P("ep", None),
        P(),
        P(None, "tp"),
        P(None, "tp"),
        P(None, "tp"),
        P("tp", None),
        P("tp"),
        P("ep", None, "tp"),
        P("ep", None, "tp"),
        P("ep"),
        P(),
        P(None, ("ep", "tp")),
        P(None, ("ep", "tp")),
        P(("ep", "tp"), None),
        P(None, "ep"),
        P(None, "ep"),
        P("ep", None),
        P(),
        P(("ep", "tp"), None),
        P(("ep", "tp"), None),
    )
    return jax.shard_map(
        shards,
        mesh=mesh,
        in_specs=placed,
        out_specs=(P(("ep", "tp"), None), P("ep", "tp"), P("ep", "tp")),
        check_vma=False,
    )
```

profile of v0, /device:TPU:0, one launch (start us, length us, event | category | flops | bytes accessed | tf_op | source)
XLA Modules:
  0.0 201.0 jit_solution(5162440769318501514)
XLA Ops:
  7.2 0.0 copy-start
  7.2 0.0 reduce-scatter.3.cloned.1.call-start
  7.2 1.1 fusion.31
  8.3 2.9 %convolution_convert_fusion.4 = bf16[16,1024]{1,0:T(8,128)(2,1)S(1)} fusion(bf16[2048,1024]{1,0:T(8,128)(2,1)} %param.22, bf16[16,2048]{1,0:T(8,128)(2,1)} %param.20, f32[2048]{0:T(1024)} %param.21, f32[16]{0:T(128)S(1)} %add_rsqrt_fusion.1), kind=kOutput, calls=%fused_computation.17 | convolution fusion | flops 67256320 | bytes 4300864 | tf_op jit(solution)/shard_map/dot_general | solution.py:75
  11.3 0.1 reshape.82
  11.4 0.0 copy-start.9
  11.4 0.0 copy-start.8
  11.4 6.4 %copy.57 = bf16[16,1024,128]{1,2,0:T(8,128)(2,1)} copy(bf16[16,1024,128]{2,1,0:T(8,128)(2,1)} %param.27) | data formatting | bytes 8388608 | tf_op args[7]
  17.8 0.0 copy-done.9
  17.8 0.1 add.75
  17.9 0.0 copy-done.8
  17.9 0.1 iota_compare_fusion.1
  18.0 2.8 %fusion.4 = f32[16,2,8,1024]{3,2,1,0:T(8,128)S(1)} fusion(bf16[16,2,8,64]{3,2,1,0:T(8,128)(2,1)S(1)} %reshape.82, bf16[16,1024,2,64]{1,3,2,0:T(8,128)(2,1)} %bitcast.71, f32[2,8]{1,0:T(2,128)S(1)} %add.75), kind=kOutput, calls=%fused_computation.13 | convolution fusion | flops 34078720 | bytes 5275712 | tf_op jit(solution)/shard_map/bgrd,bsgd->bgrs/dot_general | solution.py:81
  20.8 1.0 copy-done.1
  21.8 0.7 fusion.18
  22.5 1.7 fusion.19
  24.1 2.8 %copy.74 = f32[16,2,8,8,1]{3,2,1,0,4:T(8,128)S(1)} copy(f32[16,2,8,8,1]{4,3,2,1,0:T(8,128)} %bitcast.73) | data formatting | bytes 16384 | tf_op jit(solution)/shard_map/squeeze | solution.py:28
  26.9 0.2 fusion.34
  27.1 2.6 %add_subtract_fusion = f32[16,2,8,8,128]{4,3,2,1,0:T(8,128)} fusion(f32[16,2,8,8,128]{4,3,2,1,0:T(8,128)} %fusion.19, f32[16,2,8,8,128]{4,2,3,1,0:T(8,128)S(1)} %fusion.18, f32[16,2,8,8]{3,2,1,0:T(8,128)S(1)} %fusion.34), kind=kLoop, calls=%fused_computation.36 | loop fusion | flops 524288 | bytes 3153920 | tf_op jit(solution)/shard_map/sub | solution.py:34
  29.7 2.4 %reshape.85 = f32[16,2,8,1024]{3,2,1,0:T(8,128)} reshape(f32[16,2,8,8,128]{4,3,2,1,0:T(8,128)} %add_subtract_fusion) | data formatting | bytes 2097152 | tf_op jit(solution)/shard_map/reshape | solution.py:34
  32.1 6.5 %copy.62 = bf16[16,1024,128]{1,2,0:T(8,128)(2,1)} copy(bf16[16,1024,128]{2,1,0:T(8,128)(2,1)} %param.28) | data formatting | bytes 8388608 | tf_op args[8]
  38.6 0.0 copy-done.2
  38.6 0.0 copy-start.3
  38.6 0.0 copy-start.5
  38.6 3.8 %convolution_convert_fusion.3 = bf16[16,2,8,64]{3,2,1,0:T(8,128)(2,1)S(1)} fusion(bf16[16,1024,2,64]{1,3,2,0:T(8,128)(2,1)} %bitcast.72, f32[16,2,8,1024]{3,2,1,0:T(8,128)} %reshape.85, f32[16,2,8,1024]{3,2,1,0:T(8,128)S(1)} %copy-done.2, pred[16,1024]{1,0:T(8,128)(4,1)S(1)} %iota_compare_fusion.1), kind=kOutput, calls=%fused_computation.16 | convolution fusion | flops 36454400 | bytes 6340608 | tf_op jit(solution)/shard_map/bgrs,bsgd->bgrd/dot_general | solution.py:92
  42.4 0.1 reshape.87
  42.5 3.5 %convolution_convert_fusion.2 = bf16[16,2048]{1,0:T(8,128)(2,1)} fusion(bf16[16,1024]{1,0:T(8,128)(2,1)S(1)} %reshape.87, bf16[1024,2048]{1,0:T(8,128)(2,1)} %param.25), kind=kOutput, calls=%fused_computation.7 | convolution fusion | flops 67141632 | bytes 4292608 | tf_op jit(solution)/shard_map/dot_general | solution.py:96
  46.0 0.0 reduce-scatter.3.cloned.1.call-update
  46.0 0.0 copy-done.7
  46.0 0.1 fusion.6
  46.2 0.1 copy.64
  46.2 0.1 copy.63
  46.3 0.0 copy-done.6
  46.4 10.1 %reduce-scatter.3.cloned.1.call-done = bf16[8,2048]{1,0:T(8,128)(2,1)} async-done(((bf16[16,2048]{1,0:T(8,128)(2,1)}), bf16[8,2048]{1,0:T(8,128)(2,1)}) %reduce-scatter.3.cloned.1.call-update) | async-done | bytes 32784 | tf_op jit(solution)/shard_map/reduce_scatter | solution.py:97
  56.4 0.0 copy-done.3
  56.4 0.9 fusion.37
  57.3 0.0 copy-done.5
  57.3 0.1 fusion.39
  57.4 44.0 %all_gather.3 = bf16[128,2048]{1,0:T(8,128)(2,1)S(1)} all-gather(bf16[8,2048]{1,0:T(8,128)(2,1)S(1)} %fusion.39), channel_id=1, replica_groups=mesh['ep'=16,'tp'=2] {'ep'}, dimensions={0}, use_global_device_ids=true | all-gather | bytes 557056 | tf_op jit(solution)/shard_map/all_gather | solution.py:106
  101.4 0.2 convolution_convert_fusion.1
  101.6 0.1 copy.67
  101.7 1.1 broadcast_in_dim.44
  102.7 2.6 %all-to-all-start = ((bf16[32,3,2048]{2,1,0:T(4,128)(2,1)}), bf16[32,3,2048]{2,1,0:T(4,128)(2,1)S(1)}, u32[]{:S(2)}, u32[]{:S(2)}) async-start(bf16[32,3,2048]{2,1,0:T(4,128)(2,1)} %bitcast.11), calls=%async_computation.1 | async-start | bytes 1048576 | tf_op jit(solution)/shard_map/all_to_all | solution.py:129
  105.3 0.2 reduce-scatter.5.cloned.1.call-start
  105.6 0.2 fusion.10
  105.8 2.2 %fusion.65 = f32[128,448]{0,1:T(8,128)S(1)} fusion(bf16[128,2048]{1,0:T(8,128)(2,1)S(1)} %all_gather.3, bf16[2048,448]{0,1:T(8,128)(2,1)} %param.34), kind=kOutput, calls=%fused_computation.91 | convolution fusion | flops 234881024 | bytes 2588672 | tf_op jit(solution)/shard_map/dot_general | solution.py:109
  108.0 4.0 %convolution_multiply_fusion = f32[128,2048]{1,0:T(8,128)} fusion(bf16[448,2048]{1,0:T(8,128)(2,1)S(1)} %copy-done, bf16[128,2048]{1,0:T(8,128)(2,1)S(1)} %all_gather.3, bf16[2048,448]{0,1:T(8,128)(2,1)} %param.35, f32[128]{0:T(128)S(1)} %fusion.10, f32[128,448]{0,1:T(8,128)S(1)} %fusion.65), kind=kOutput, calls=%fused_computation.2 | convolution fusion | flops 470368256 | bytes 5472768 | tf_op jit(solution)/shard_map/dot_general | solution.py:113
  112.0 0.0 reduce-scatter.5.cloned.1.call-update
  112.0 8.9 %all-to-all-done = bf16[32,3,2048]{2,1,0:T(4,128)(2,1)S(1)} async-done(((bf16[32,3,2048]{2,1,0:T(4,128)(2,1)}), bf16[32,3,2048]{2,1,0:T(4,128)(2,1)S(1)}, u32[]{:S(2)}, u32[]{:S(2)}) %all-to-all-start) | async-done | bytes 393248 | tf_op jit(solution)/shard_map/all_to_all | solution.py:129
  121.0 0.3 reshape.89
  121.3 4.4 %fusion.64 = f32[96,1792]{1,0:T(8,128)S(1)} fusion(bf16[96,2048]{1,0:T(8,128)(2,1)S(1)} %reshape.89, bf16[2048,1792]{1,0:T(8,128)(2,1)} %param.31), kind=kOutput, calls=%fused_computation.90 | convolution fusion | flops 704643072 | bytes 8421376 | tf_op jit(solution)/shard_map/dot_general | solution.py:132
  125.7 0.0 copy-start.10
  125.7 0.0 copy-start.4
  125.7 7.8 %convolution_convert_fusion = bf16[96,2048]{1,0:T(8,128)(2,1)S(1)} fusion(bf16[1792,2048]{1,0:T(8,128)(2,1)} %param.33, bf16[96,2048]{1,0:T(8,128)(2,1)S(1)} %reshape.89, bf16[2048,1792]{1,0:T(8,128)(2,1)} %param.32, f32[96,1792]{1,0:T(8,128)S(1)} %fusion.64), kind=kOutput, calls=%fused_computation.5 | convolution fusion | flops 1410514944 | bytes 16154624 | tf_op jit(solution)/shard_map/dot_general | solution.py:135
  133.5 1.0 convert_element_type.98
  134.6 2.9 %all-to-all-start.1 = ((bf16[32,3,2048]{2,1,0:T(4,128)(2,1)}), bf16[32,3,2048]{2,1,0:T(4,128)(2,1)S(1)}, u32[]{:S(2)}, u32[]{:S(2)}) async-start(bf16[32,3,2048]{2,1,0:T(4,128)(2,1)} %convert_element_type.98), calls=%async_computation.2 | async-start | bytes 1048576 | tf_op jit(solution)/shard_map/all_to_all | solution.py:138
  137.5 0.0 copy-done.10
  137.5 0.1 copy.65
  137.6 1.9 convolution_convert_fusion.5
  139.5 1.9 convolution_convert_fusion.6
  141.4 13.6 %all-to-all-done.1 = bf16[32,3,2048]{2,1,0:T(4,128)(2,1)S(1)} async-done(((bf16[32,3,2048]{2,1,0:T(4,128)(2,1)}), bf16[32,3,2048]{2,1,0:T(4,128)(2,1)S(1)}, u32[]{:S(2)}, u32[]{:S(2)}) %all-to-all-start.1) | async-done | bytes 393248 | tf_op jit(solution)/shard_map/all_to_all | solution.py:138
  154.9 0.3 convert_reduce_fusion
  155.2 37.3 %reduce-scatter.5.cloned.1.call-done = f32[8,2048]{1,0:T(8,128)} async-done(((f32[128,2048]{1,0:T(8,128)}), f32[8,2048]{1,0:T(8,128)}) %reduce-scatter.5.cloned.1.call-update) | async-done | bytes 65552 | tf_op jit(solution)/shard_map/reduce_scatter | solution.py:115
  192.5 1.7 fusion.3
  (13 shorter events, 0.1 us)
Async XLA Ops:
  7.2 100.8 %copy-start = (bf16[448,2048]{1,0:T(8,128)(2,1)S(1)}, bf16[448,2048]{1,0:T(8,128)(2,1)}, u32[]{:S(2)}) copy-start(bf16[448,2048]{1,0:T(8,128)(2,1)} %param.36) | copy-start | bytes 5505028
  7.2 49.2 %reduce-scatter.3.cloned.1.call-start = ((), (), s32[]{:S(2)}) async-start(), calls=%async_computation.4 | async-start | bytes 98304 | tf_op jit(solution)/shard_map/reduce_scatter | solution.py:97
  11.4 6.4 %copy-start.9 = (f32[16]{0:T(128)S(1)}, f32[16]{0:T(128)}, u32[]{:S(2)}) copy-start(f32[16]{0:T(128)} %param.26) | copy-start | bytes 196
  11.4 6.5 %copy-start.8 = (s32[16]{0:T(128)S(1)}, s32[16]{0:T(128)}, u32[]{:S(2)}) copy-start(s32[16]{0:T(128)} %param.29) | copy-start | bytes 196
  20.8 1.0 copy-start.1
  32.1 6.5 %copy-start.2 = (f32[16,2,8,1024]{3,2,1,0:T(8,128)S(1)}, f32[16,2,8,1024]{3,2,1,0:T(8,128)}, u32[]{:S(2)}) copy-start(f32[16,2,8,1024]{3,2,1,0:T(8,128)} %copy-done.1) | copy-start | bytes 3145732
  38.6 7.4 %copy-start.7 = (s32[8,2]{0,1:T(2,128)S(1)}, s32[8,2]{0,1:T(2,128)}, u32[]{:S(2)}) copy-start(s32[8,2]{0,1:T(2,128)} %param.38) | copy-start | bytes 196
  38.6 7.7 %copy-start.6 = (bf16[2048]{0:T(1024)(128)(2,1)S(1)}, bf16[2048]{0:T(1024)(128)(2,1)}, u32[]{:S(2)}) copy-start(bf16[2048]{0:T(1024)(128)(2,1)} %param.37) | copy-start | bytes 12292
  38.6 17.8 %copy-start.3 = (bf16[16,2048]{1,0:T(8,128)(2,1)S(1)}, bf16[16,2048]{1,0:T(8,128)(2,1)}, u32[]{:S(2)}) copy-start(bf16[16,2048]{1,0:T(8,128)(2,1)} %param.20) | copy-start | bytes 196612
  38.6 18.7 %copy-start.5 = (f32[2048]{0:T(1024)S(1)}, f32[2048]{0:T(1024)}, u32[]{:S(2)}) copy-start(f32[2048]{0:T(1024)} %param.30) | copy-start | bytes 24580
  102.7 18.2 %all-to-all-start = ((bf16[32,3,2048]{2,1,0:T(4,128)(2,1)}), bf16[32,3,2048]{2,1,0:T(4,128)(2,1)S(1)}, u32[]{:S(2)}, u32[]{:S(2)}) async-start(bf16[32,3,2048]{2,1,0:T(4,128)(2,1)} %bitcast.11), calls=%async_computation.1 | async-start | bytes 1048576 | tf_op jit(solution)/shard_map/all_to_all | solution.py:129
  105.3 87.1 %reduce-scatter.5.cloned.1.call-start = ((), (), s32[]{:S(2)}) async-start(), calls=%async_computation.5 | async-start | bytes 1114112 | tf_op jit(solution)/shard_map/reduce_scatter | solution.py:115
  125.7 11.8 %copy-start.10 = (bf16[8,2]{0,1:T(2,128)(2,1)S(1)}, bf16[8,2]{0,1:T(2,128)(2,1)}, u32[]{:S(2)}) copy-start(bf16[8,2]{0,1:T(2,128)(2,1)} %param.39) | copy-start | bytes 100
  125.7 11.9 %copy-start.4 = (f32[2048]{0:T(1024)S(1)}, f32[2048]{0:T(1024)}, u32[]{:S(2)}) copy-start(f32[2048]{0:T(1024)} %param.21) | copy-start | bytes 24580
  134.6 20.3 %all-to-all-start.1 = ((bf16[32,3,2048]{2,1,0:T(4,128)(2,1)}), bf16[32,3,2048]{2,1,0:T(4,128)(2,1)S(1)}, u32[]{:S(2)}, u32[]{:S(2)}) async-start(bf16[32,3,2048]{2,1,0:T(4,128)(2,1)} %convert_element_type.98), calls=%async_computation.2 | async-start | bytes 1048576 | tf_op jit(solution)/shard_map/all_to_all | solution.py:138
Sparse Core Ops, SparseCore 0:
  46.1 10.2 reduce-scatter.2
  112.2 80.2 reduce-scatter.4
where the time goes:
time: 202 us; the launch traced here: 201 us
  waiting for transfers between devices  69.9 us (35%)
  blocking collectives  44 us (22%)
  matrix products  39.3 us (19%)
  local copies, waits for them, and re-layouts  22.1 us (11%)
  between operations  14.3 us (7%)
  starting transfers between devices  5.75 us (3%)
  other arithmetic  5.72 us (3%)
    all_gather x1, blocking collectives, shards(): piece = lax.all_gather(normed_two, 'ep', axis=0, tiled=True)  44 us
    reduce_scatter x1, waiting for transfers between devices, shards(): lax.psum_scatter(dense_terms, 'ep', scatter_dimension=0, tiled=True)  37.3 us
    unnamed x25, local copies, waits for them, and re-layouts  13.9 us
    all_to_all x1, waiting for transfers between devices, shards(): lax.all_to_all(expert_result.astype(jnp.bfloat16), ('ep', 'tp'), split_ax...  13.6 us
    reduce_scatter x1, waiting for transfers between devices, shards(): lax.psum_scatter(partial_value.astype(jnp.bfloat16), 'tp', scatter_dimens...  10.1 us
    all_to_all x1, waiting for transfers between devices, shards(): lax.all_to_all(outgoing, ('ep', 'tp'), split_axis=0, concat_axis=0, tiled...  8.92 us
    dot_general x1, matrix products, shards(): jnp.dot(expert_hidden, expert_down, preferred_element_type=jnp.float32)  7.84 us
    dot_general x1, matrix products, shards(): jnp.dot(slot_rows, expert_gate, preferred_element_type=jnp.float32)  4.37 us
  transfers between devices with their start and end apart: 4, of which 4 were waited for; matrix products, arithmetic and copies ran while one was open for 12% of the time, Pallas kernels for 0%

commit v1 on v0

--- a/solution.py
+++ b/solution.py
@@ -7,6 +7,17 @@
 EXPERTS = 8
 TOP = 2
 EPSILON = 1e-06
+
+
+def gather_by_hops(block, axis, along):
+    size = lax.axis_size(axis)
+    right = [(i, (i + 1) % size) for i in range(size)]
+    parts = [block]
+    for far in range(1, size):
+        parts = [lax.ppermute(parts[0], axis, right), *parts]
+    whole = jnp.concatenate(parts, axis=along)
+    shift = (lax.axis_index(axis) + 1) * parts[-1].shape[along]
+    return jnp.roll(whole, shift, axis=along)
 
 
 def normed_rows(values, gain):
@@ -103,7 +114,7 @@
     middle = (own_rows.astype(jnp.float32) + attn_sum).astype(jnp.bfloat16)
     normed_two = normed_rows(middle, norm_ffn)
     width = normed_two.shape[1]
-    piece = lax.all_gather(normed_two, "ep", axis=0, tiled=True)
+    piece = gather_by_hops(normed_two, "ep", 0)
     mix_gate = jax.nn.sigmoid(jnp.dot(piece, dense_mix, preferred_element_type=jnp.float32))
     dense_hidden = (
         jax.nn.silu(jnp.dot(piece, dense_gate_w, preferred_element_type=jnp.float32))

time: 202 us -> 299 us (1.48)
  waiting for transfers between devices: 69.9 us -> 170 us
  blocking collectives: 44 us -> 0 us
  local copies, waits for them, and re-layouts: 22.1 us -> 50.5 us
  starting transfers between devices: 5.75 us -> 13.8 us
    ppermute x0 -> x15, waiting for transfers between devices: none -> 103 us  [gather_by_hops(): parts = [lax.ppermute(parts[0], axis, right), *parts]]
    all_gather x1 -> x0, blocking collectives: 44 us -> none  [shards(): piece = lax.all_gather(normed_two, 'ep', axis=0, tiled=True)]
    unnamed x25 -> x89, local copies, waits for them, and re-layouts: 13.9 us -> 42.3 us
    all_to_all x1, waiting for transfers between devices: 8.92 us -> 0.01 us  [shards(): lax.all_to_all(outgoing, ('ep', 'tp'), split_axis=0, concat_axis=0, tiled...]
    reduce_scatter x1, waiting for transfers between devices: 37.3 us -> 43.1 us  [shards(): lax.psum_scatter(dense_terms, 'ep', scatter_dimension=0, tiled=True)]
    all_to_all x1, starting transfers between devices: 2.6 us -> 5.98 us  [shards(): lax.all_to_all(outgoing, ('ep', 'tp'), split_axis=0, concat_axis=0, tiled...]
  transfers between devices with their start and end apart: 4 -> 19, of which waited for: 4 -> 17; matrix products, arithmetic and copies ran while one was open for 12% -> 17% of each run, Pallas kernels for 0% -> 0%
where the time goes in v1:
time: 299 us; the launch traced here: 296 us
  waiting for transfers between devices  170 us (57%)
  local copies, waits for them, and re-layouts  50.5 us (17%)
  matrix products  40.7 us (14%)
  between operations  14.4 us (5%)
  starting transfers between devices  13.8 us (5%)
  other arithmetic  7.18 us (2%)
    ppermute x15, waiting for transfers between devices, gather_by_hops(): parts = [lax.ppermute(parts[0], axis, right), *parts]  103 us
    reduce_scatter x1, waiting for transfers between devices, shards(): lax.psum_scatter(dense_terms, 'ep', scatter_dimension=0, tiled=True)  43.1 us
    unnamed x89, local copies, waits for them, and re-layouts  42.3 us
    all_to_all x1, waiting for transfers between devices, shards(): lax.all_to_all(expert_result.astype(jnp.bfloat16), ('ep', 'tp'), split_ax...  13.6 us
    reduce_scatter x1, waiting for transfers between devices, shards(): lax.psum_scatter(partial_value.astype(jnp.bfloat16), 'tp', scatter_dimens...  10.4 us
    dot_general x1, matrix products, shards(): jnp.dot(expert_hidden, expert_down, preferred_element_type=jnp.float32)  7.84 us
    all_to_all x1, starting transfers between devices, shards(): lax.all_to_all(outgoing, ('ep', 'tp'), split_axis=0, concat_axis=0, tiled...  5.98 us
  transfers between devices with their start and end apart: 19, of which 17 were waited for; matrix products, arithmetic and copies ran while one was open for 17% of the time, Pallas kernels for 0%

profile of v1, /device:TPU:0, one launch (start us, length us, event | category | flops | bytes accessed | tf_op | source)
XLA Modules:
  0.0 296.2 jit_solution(12173232334426916049)
XLA Ops:
  7.2 1.1 fusion.30
  8.8 2.9 convolution_convert_fusion.4
  11.9 6.4 %copy.57 = bf16[16,1024,128]{1,2,0:T(8,128)(2,1)} copy(bf16[16,1024,128]{2,1,0:T(8,128)(2,1)} %param.27) | data formatting | bytes 8388608 | tf_op args[7]
  18.5 2.8 fusion.4
  21.4 1.0 copy-done.1
  23.0 1.7 fusion.18
  24.7 2.8 copy.74
  27.7 2.6 add_subtract_fusion
  30.3 2.4 reshape.85
  32.7 6.5 %copy.62 = bf16[16,1024,128]{1,2,0:T(8,128)(2,1)} copy(bf16[16,1024,128]{2,1,0:T(8,128)(2,1)} %param.28) | data formatting | bytes 8388608 | tf_op args[8]
  39.2 3.8 %convolution_convert_fusion.3 = bf16[16,2,8,64]{3,2,1,0:T(8,128)(2,1)S(1)} fusion(bf16[16,1024,2,64]{1,3,2,0:T(8,128)(2,1)} %bitcast.69, f32[16,2,8,1024]{3,2,1,0:T(8,128)} %reshape.85, f32[16,2,8,1024]{3,2,1,0:T(8,128)S(1)} %copy-done.2, pred[16,1024]{1,0:T(8,128)(4,1)S(1)} %iota_compare_fusion.1), kind=kOutput, calls=%fused_computation.14 | convolution fusion | flops 36454400 | bytes 6340608 | tf_op jit(solution)/shard_map/bgrs,bsgd->bgrd/dot_general | solution.py:103
  43.1 3.5 %convolution_convert_fusion.2 = bf16[16,2048]{1,0:T(8,128)(2,1)} fusion(bf16[16,1024]{1,0:T(8,128)(2,1)S(1)} %reshape.87, bf16[1024,2048]{1,0:T(8,128)(2,1)} %param.25), kind=kOutput, calls=%fused_computation.7 | convolution fusion | flops 67141632 | bytes 4292608 | tf_op jit(solution)/shard_map/dot_general | solution.py:107
  46.6 10.4 %reduce-scatter.3.cloned.1.call-done = bf16[8,2048]{1,0:T(8,128)(2,1)} async-done(((bf16[16,2048]{1,0:T(8,128)(2,1)}), bf16[8,2048]{1,0:T(8,128)(2,1)}) %reduce-scatter.3.cloned.1.call-update) | async-done | bytes 32784 | tf_op jit(solution)/shard_map/reduce_scatter | solution.py:108
  57.0 0.9 fusion.40
  58.5 1.7 collective-permute-start
  60.2 5.8 %collective-permute-done = bf16[8,2048]{1,0:T(8,128)(2,1)S(1)} collective-permute-done((bf16[8,2048]{1,0:T(8,128)(2,1)S(1)}, bf16[8,2048]{1,0:T(8,128)(2,1)S(1)}, u32[]{:S(2)}, u32[]{:S(2)}) %collective-permute-start) | collective-permute-done | bytes 32800 | tf_op jit(solution)/shard_map/ppermute | solution.py:17
  66.0 7.5 %collective-permute-done.1 = bf16[8,2048]{1,0:T(8,128)(2,1)S(1)} collective-permute-done((bf16[8,2048]{1,0:T(8,128)(2,1)S(1)}, bf16[8,2048]{1,0:T(8,128)(2,1)S(1)}, u32[]{:S(2)}, u32[]{:S(2)}) %collective-permute-start.1) | collective-permute-done | bytes 32800 | tf_op jit(solution)/shard_map/ppermute | solution.py:17
  74.2 7.5 %collective-permute-done.2 = bf16[8,2048]{1,0:T(8,128)(2,1)S(1)} collective-permute-done((bf16[8,2048]{1,0:T(8,128)(2,1)S(1)}, bf16[8,2048]{1,0:T(8,128)(2,1)S(1)}, u32[]{:S(2)}, u32[]{:S(2)}) %collective-permute-start.2) | collective-permute-done | bytes 32800 | tf_op jit(solution)/shard_map/ppermute | solution.py:17
  82.3 7.5 %collective-permute-done.3 = bf16[8,2048]{1,0:T(8,128)(2,1)S(1)} collective-permute-done((bf16[8,2048]{1,0:T(8,128)(2,1)S(1)}, bf16[8,2048]{1,0:T(8,128)(2,1)S(1)}, u32[]{:S(2)}, u32[]{:S(2)}) %collective-permute-start.3) | collective-permute-done | bytes 32800 | tf_op jit(solution)/shard_map/ppermute | solution.py:17
  90.4 7.5 %collective-permute-done.4 = bf16[8,2048]{1,0:T(8,128)(2,1)S(1)} collective-permute-done((bf16[8,2048]{1,0:T(8,128)(2,1)S(1)}, bf16[8,2048]{1,0:T(8,128)(2,1)S(1)}, u32[]{:S(2)}, u32[]{:S(2)}) %collective-permute-start.4) | collective-permute-done | bytes 32800 | tf_op jit(solution)/shard_map/ppermute | solution.py:17
  98.5 7.5 %collective-permute-done.5 = bf16[8,2048]{1,0:T(8,128)(2,1)S(1)} collective-permute-done((bf16[8,2048]{1,0:T(8,128)(2,1)S(1)}, bf16[8,2048]{1,0:T(8,128)(2,1)S(1)}, u32[]{:S(2)}, u32[]{:S(2)}) %collective-permute-start.5) | collective-permute-done | bytes 32800 | tf_op jit(solution)/shard_map/ppermute | solution.py:17
  106.6 7.5 %collective-permute-done.6 = bf16[8,2048]{1,0:T(8,128)(2,1)S(1)} collective-permute-done((bf16[8,2048]{1,0:T(8,128)(2,1)S(1)}, bf16[8,2048]{1,0:T(8,128)(2,1)S(1)}, u32[]{:S(2)}, u32[]{:S(2)}) %collective-permute-start.6) | collective-permute-done | bytes 32800 | tf_op jit(solution)/shard_map/ppermute | solution.py:17
  114.7 7.5 %collective-permute-done.7 = bf16[8,2048]{1,0:T(8,128)(2,1)S(1)} collective-permute-done((bf16[8,2048]{1,0:T(8,128)(2,1)S(1)}, bf16[8,2048]{1,0:T(8,128)(2,1)S(1)}, u32[]{:S(2)}, u32[]{:S(2)}) %collective-permute-start.7) | collective-permute-done | bytes 32800 | tf_op jit(solution)/shard_map/ppermute | solution.py:17
  122.8 7.5 %collective-permute-done.8 = bf16[8,2048]{1,0:T(8,128)(2,1)S(1)} collective-permute-done((bf16[8,2048]{1,0:T(8,128)(2,1)S(1)}, bf16[8,2048]{1,0:T(8,128)(2,1)S(1)}, u32[]{:S(2)}, u32[]{:S(2)}) %collective-permute-start.8) | collective-permute-done | bytes 32800 | tf_op jit(solution)/shard_map/ppermute | solution.py:17
  131.0 7.5 %collective-permute-done.9 = bf16[8,2048]{1,0:T(8,128)(2,1)S(1)} collective-permute-done((bf16[8,2048]{1,0:T(8,128)(2,1)S(1)}, bf16[8,2048]{1,0:T(8,128)(2,1)S(1)}, u32[]{:S(2)}, u32[]{:S(2)}) %collective-permute-start.9) | collective-permute-done | bytes 32800 | tf_op jit(solution)/shard_map/ppermute | solution.py:17
  139.1 7.5 %collective-permute-done.10 = bf16[8,2048]{1,0:T(8,128)(2,1)S(1)} collective-permute-done((bf16[8,2048]{1,0:T(8,128)(2,1)S(1)}, bf16[8,2048]{1,0:T(8,128)(2,1)S(1)}, u32[]{:S(2)}, u32[]{:S(2)}) %collective-permute-start.10) | collective-permute-done | bytes 32800 | tf_op jit(solution)/shard_map/ppermute | solution.py:17
  146.6 7.5 %collective-permute-done.11 = bf16[8,2048]{1,0:T(8,128)(2,1)S(1)} collective-permute-done((bf16[8,2048]{1,0:T(8,128)(2,1)S(1)}, bf16[8,2048]{1,0:T(8,128)(2,1)S(1)}, u32[]{:S(2)}, u32[]{:S(2)}) %collective-permute-start.11) | collective-permute-done | bytes 32800 | tf_op jit(solution)/shard_map/ppermute | solution.py:17
  154.2 7.4 %collective-permute-done.12 = bf16[8,2048]{1,0:T(8,128)(2,1)S(1)} collective-permute-done((bf16[8,2048]{1,0:T(8,128)(2,1)S(1)}, bf16[8,2048]{1,0:T(8,128)(2,1)S(1)}, u32[]{:S(2)}, u32[]{:S(2)}) %collective-permute-start.12) | collective-permute-done | bytes 32800 | tf_op jit(solution)/shard_map/ppermute | solution.py:17
  162.4 6.7 %collective-permute-done.13 = bf16[8,2048]{1,0:T(8,128)(2,1)S(1)} collective-permute-done((bf16[8,2048]{1,0:T(8,128)(2,1)S(1)}, bf16[8,2048]{1,0:T(8,128)(2,1)S(1)}, u32[]{:S(2)}, u32[]{:S(2)}) %collective-permute-start.13) | collective-permute-done | bytes 32800 | tf_op jit(solution)/shard_map/ppermute | solution.py:17
  169.4 1.0 broadcast_in_dim.44
  170.5 6.0 %all-to-all-start = ((bf16[32,3,2048]{2,1,0:T(4,128)(2,1)}), bf16[32,3,2048]{2,1,0:T(4,128)(2,1)S(1)}, u32[]{:S(2)}, u32[]{:S(2)}) async-start(bf16[32,3,2048]{2,1,0:T(4,128)(2,1)} %bitcast.11), calls=%async_computation.1 | async-start | bytes 1048576 | tf_op jit(solution)/shard_map/all_to_all | solution.py:140
  176.8 0.8 constant_dynamic-update-slice_fusion.31
  177.5 0.8 constant_dynamic-update-slice_fusion.30
  178.3 0.8 constant_dynamic-update-slice_fusion.29
  179.0 0.8 constant_dynamic-update-slice_fusion.28
  179.8 0.8 constant_dynamic-update-slice_fusion.27
  180.6 0.8 constant_dynamic-update-slice_fusion.26
  181.3 0.8 constant_dynamic-update-slice_fusion.25
  182.1 0.8 constant_dynamic-update-slice_fusion.24
  182.8 0.8 constant_dynamic-update-slice_fusion.23
  183.6 0.8 constant_dynamic-update-slice_fusion.22
  184.4 0.8 constant_dynamic-update-slice_fusion.21
  185.1 0.8 constant_dynamic-update-slice_fusion.20
  185.9 0.8 constant_dynamic-update-slice_fusion.19
  186.6 0.8 constant_dynamic-update-slice_fusion.18
  188.1 0.8 constant_dynamic-update-slice_fusion.15
  188.9 0.8 constant_dynamic-update-slice_fusion.14
  189.7 0.8 constant_dynamic-update-slice_fusion.13
  190.4 0.8 constant_dynamic-update-slice_fusion.12
  191.2 0.8 constant_dynamic-update-slice_fusion.11
  191.9 0.8 constant_dynamic-update-slice_fusion.10
  192.7 0.8 constant_dynamic-update-slice_fusion.9
  199.5 0.9 fusion.9
  200.5 2.9 fusion.24
  203.3 4.0 %convolution_multiply_fusion = f32[128,2048]{1,0:T(8,128)} fusion(bf16[448,2048]{1,0:T(8,128)(2,1)S(1)} %copy-done, f32[128]{0:T(128)S(1)} %fusion.9, f32[128,448]{0,1:T(8,128)} %fusion.24, bf16[2048,448]{0,1:T(8,128)(2,1)} %param.34, bf16[256,2048]{1,0:T(8,128)(2,1)S(1)} %constant_dynamic-update-slice_fusion, s32[]{:T(128)S(6)} %select_n.42), kind=kOutput, calls=%fused_computation.2 | convolution fusion | flops 470368256 | bytes 5472772 | tf_op jit(solution)/shard_map/dot_general | solution.py:124
  207.8 4.4 %fusion.71 = f32[96,1792]{1,0:T(8,128)S(1)} fusion(bf16[96,2048]{1,0:T(8,128)(2,1)S(1)} %reshape.89, bf16[2048,1792]{1,0:T(8,128)(2,1)} %param.31), kind=kOutput, calls=%fused_computation.124 | convolution fusion | flops 704643072 | bytes 8421376 | tf_op jit(solution)/shard_map/dot_general | solution.py:143
  212.2 7.8 %convolution_convert_fusion = bf16[96,2048]{1,0:T(8,128)(2,1)S(1)} fusion(bf16[1792,2048]{1,0:T(8,128)(2,1)} %param.33, bf16[96,2048]{1,0:T(8,128)(2,1)S(1)} %reshape.89, bf16[2048,1792]{1,0:T(8,128)(2,1)} %param.32, f32[96,1792]{1,0:T(8,128)S(1)} %fusion.71), kind=kOutput, calls=%fused_computation.5 | convolution fusion | flops 1410514944 | bytes 16154624 | tf_op jit(solution)/shard_map/dot_general | solution.py:146
  220.0 1.0 convert_element_type.98
  221.0 5.8 %all-to-all-start.1 = ((bf16[32,3,2048]{2,1,0:T(4,128)(2,1)}), bf16[32,3,2048]{2,1,0:T(4,128)(2,1)S(1)}, u32[]{:S(2)}, u32[]{:S(2)}) async-start(bf16[32,3,2048]{2,1,0:T(4,128)(2,1)} %convert_element_type.98), calls=%async_computation.2 | async-start | bytes 1048576 | tf_op jit(solution)/shard_map/all_to_all | solution.py:149
  227.0 1.9 convolution_convert_fusion.5
  228.9 1.9 convolution_convert_fusion.6
  230.8 13.6 %all-to-all-done.1 = bf16[32,3,2048]{2,1,0:T(4,128)(2,1)S(1)} async-done(((bf16[32,3,2048]{2,1,0:T(4,128)(2,1)}), bf16[32,3,2048]{2,1,0:T(4,128)(2,1)S(1)}, u32[]{:S(2)}, u32[]{:S(2)}) %all-to-all-start.1) | async-done | bytes 393248 | tf_op jit(solution)/shard_map/all_to_all | solution.py:149
  244.6 43.1 %reduce-scatter.5.cloned.1.call-done = f32[8,2048]{1,0:T(8,128)} async-done(((f32[128,2048]{1,0:T(8,128)}), f32[8,2048]{1,0:T(8,128)}) %reduce-scatter.5.cloned.1.call-update) | async-done | bytes 65552 | tf_op jit(solution)/shard_map/reduce_scatter | solution.py:126
  287.7 1.7 fusion.3
  (108 shorter events, 16.9 us)
Async XLA Ops:
  7.2 196.2 %copy-start = (bf16[448,2048]{1,0:T(8,128)(2,1)S(1)}, bf16[448,2048]{1,0:T(8,128)(2,1)}, u32[]{:S(2)}) copy-start(bf16[448,2048]{1,0:T(8,128)(2,1)} %param.36) | copy-start | bytes 5505028
  7.2 49.8 %reduce-scatter.3.cloned.1.call-start = ((), (), s32[]{:S(2)}) async-start(), calls=%async_computation.4 | async-start | bytes 98304 | tf_op jit(solution)/shard_map/reduce_scatter | solution.py:108
  8.3 0.5 copy-start.20
  11.9 6.4 %copy-start.26 = (f32[16]{0:T(128)S(1)}, f32[16]{0:T(128)}, u32[]{:S(2)}) copy-start(f32[16]{0:T(128)} %param.26) | copy-start | bytes 196
  11.9 6.5 %copy-start.25 = (s32[16]{0:T(128)S(1)}, s32[16]{0:T(128)}, u32[]{:S(2)}) copy-start(s32[16]{0:T(128)} %param.29) | copy-start | bytes 196
  21.3 1.0 copy-start.1
  32.7 6.5 %copy-start.2 = (f32[16,2,8,1024]{3,2,1,0:T(8,128)S(1)}, f32[16,2,8,1024]{3,2,1,0:T(8,128)}, u32[]{:S(2)}) copy-start(f32[16,2,8,1024]{3,2,1,0:T(8,128)} %copy-done.1) | copy-start | bytes 3145732
  39.2 17.8 %copy-start.3 = (bf16[16,2048]{1,0:T(8,128)(2,1)S(1)}, bf16[16,2048]{1,0:T(8,128)(2,1)}, u32[]{:S(2)}) copy-start(bf16[16,2048]{1,0:T(8,128)(2,1)} %param.20) | copy-start | bytes 196612
  39.2 19.2 %copy-start.18 = (f32[2048]{0:T(1024)S(1)}, f32[2048]{0:T(1024)}, u32[]{:S(2)}) copy-start(f32[2048]{0:T(1024)} %param.30) | copy-start | bytes 24580
  39.2 107.4 %copy-start.23 = (s32[8,2]{0,1:T(2,128)S(1)}, s32[8,2]{0,1:T(2,128)}, u32[]{:S(2)}) copy-start(s32[8,2]{0,1:T(2,128)} %param.38) | copy-start | bytes 196
  39.2 122.4 %copy-start.22 = (bf16[2048]{0:T(1024)(128)(2,1)S(1)}, bf16[2048]{0:T(1024)(128)(2,1)}, u32[]{:S(2)}) copy-start(bf16[2048]{0:T(1024)(128)(2,1)} %param.37) | copy-start | bytes 12292
  57.9 0.5 copy-start.19
  58.5 7.5 %collective-permute-start = (bf16[8,2048]{1,0:T(8,128)(2,1)S(1)}, bf16[8,2048]{1,0:T(8,128)(2,1)S(1)}, u32[]{:S(2)}, u32[]{:S(2)}) collective-permute-start(bf16[8,2048]{1,0:T(8,128)(2,1)S(1)} %fusion.42), channel_id=1, source_target_pairs={{0,2},{2,4},{4,6},{6,8},{8,10},{10,12},{12,14},{14,16},{16,18},{18... | collective-permute-start | bytes 98312 | tf_op jit(solution)/shard_map/ppermute | solution.py:17
  66.0 7.5 %collective-permute-start.1 = (bf16[8,2048]{1,0:T(8,128)(2,1)S(1)}, bf16[8,2048]{1,0:T(8,128)(2,1)S(1)}, u32[]{:S(2)}, u32[]{:S(2)}) collective-permute-start(bf16[8,2048]{1,0:T(8,128)(2,1)S(1)} %collective-permute-done), channel_id=1, source_target_pairs={{0,2},{2,4},{4,6},{6,8},{8,10},{10,12},{12,14},{14,16},{16,18},{18... | collective-permute-start | bytes 98312 | tf_op jit(solution)/shard_map/ppermute | solution.py:17
  73.6 0.6 copy-start.4
  74.2 7.5 %collective-permute-start.2 = (bf16[8,2048]{1,0:T(8,128)(2,1)S(1)}, bf16[8,2048]{1,0:T(8,128)(2,1)S(1)}, u32[]{:S(2)}, u32[]{:S(2)}) collective-permute-start(bf16[8,2048]{1,0:T(8,128)(2,1)S(1)} %collective-permute-done.1), channel_id=1, source_target_pairs={{0,2},{2,4},{4,6},{6,8},{8,10},{10,12},{12,14},{14,16},{16,18},{18... | collective-permute-start | bytes 98312 | tf_op jit(solution)/shard_map/ppermute | solution.py:17
  81.7 0.6 copy-start.5
  82.3 7.5 %collective-permute-start.3 = (bf16[8,2048]{1,0:T(8,128)(2,1)S(1)}, bf16[8,2048]{1,0:T(8,128)(2,1)S(1)}, u32[]{:S(2)}, u32[]{:S(2)}) collective-permute-start(bf16[8,2048]{1,0:T(8,128)(2,1)S(1)} %collective-permute-done.2), channel_id=1, source_target_pairs={{0,2},{2,4},{4,6},{6,8},{8,10},{10,12},{12,14},{14,16},{16,18},{18... | collective-permute-start | bytes 98312 | tf_op jit(solution)/shard_map/ppermute | solution.py:17
  89.8 0.6 copy-start.6
  90.4 7.5 %collective-permute-start.4 = (bf16[8,2048]{1,0:T(8,128)(2,1)S(1)}, bf16[8,2048]{1,0:T(8,128)(2,1)S(1)}, u32[]{:S(2)}, u32[]{:S(2)}) collective-permute-start(bf16[8,2048]{1,0:T(8,128)(2,1)S(1)} %collective-permute-done.3), channel_id=1, source_target_pairs={{0,2},{2,4},{4,6},{6,8},{8,10},{10,12},{12,14},{14,16},{16,18},{18... | collective-permute-start | bytes 98312 | tf_op jit(solution)/shard_map/ppermute | solution.py:17
  97.9 0.6 copy-start.7
  98.5 7.5 %collective-permute-start.5 = (bf16[8,2048]{1,0:T(8,128)(2,1)S(1)}, bf16[8,2048]{1,0:T(8,128)(2,1)S(1)}, u32[]{:S(2)}, u32[]{:S(2)}) collective-permute-start(bf16[8,2048]{1,0:T(8,128)(2,1)S(1)} %collective-permute-done.4), channel_id=1, source_target_pairs={{0,2},{2,4},{4,6},{6,8},{8,10},{10,12},{12,14},{14,16},{16,18},{18... | collective-permute-start | bytes 98312 | tf_op jit(solution)/shard_map/ppermute | solution.py:17
  106.0 0.6 copy-start.8
  106.6 7.5 %collective-permute-start.6 = (bf16[8,2048]{1,0:T(8,128)(2,1)S(1)}, bf16[8,2048]{1,0:T(8,128)(2,1)S(1)}, u32[]{:S(2)}, u32[]{:S(2)}) collective-permute-start(bf16[8,2048]{1,0:T(8,128)(2,1)S(1)} %collective-permute-done.5), channel_id=1, source_target_pairs={{0,2},{2,4},{4,6},{6,8},{8,10},{10,12},{12,14},{14,16},{16,18},{18... | collective-permute-start | bytes 98312 | tf_op jit(solution)/shard_map/ppermute | solution.py:17
  114.1 0.6 copy-start.9
  114.7 7.5 %collective-permute-start.7 = (bf16[8,2048]{1,0:T(8,128)(2,1)S(1)}, bf16[8,2048]{1,0:T(8,128)(2,1)S(1)}, u32[]{:S(2)}, u32[]{:S(2)}) collective-permute-start(bf16[8,2048]{1,0:T(8,128)(2,1)S(1)} %collective-permute-done.6), channel_id=1, source_target_pairs={{0,2},{2,4},{4,6},{6,8},{8,10},{10,12},{12,14},{14,16},{16,18},{18... | collective-permute-start | bytes 98312 | tf_op jit(solution)/shard_map/ppermute | solution.py:17
  122.2 0.6 copy-start.10
  122.8 7.5 %collective-permute-start.8 = (bf16[8,2048]{1,0:T(8,128)(2,1)S(1)}, bf16[8,2048]{1,0:T(8,128)(2,1)S(1)}, u32[]{:S(2)}, u32[]{:S(2)}) collective-permute-start(bf16[8,2048]{1,0:T(8,128)(2,1)S(1)} %collective-permute-done.7), channel_id=1, source_target_pairs={{0,2},{2,4},{4,6},{6,8},{8,10},{10,12},{12,14},{14,16},{16,18},{18... | collective-permute-start | bytes 98312 | tf_op jit(solution)/shard_map/ppermute | solution.py:17
  130.4 0.6 copy-start.11
  131.0 7.5 %collective-permute-start.9 = (bf16[8,2048]{1,0:T(8,128)(2,1)S(1)}, bf16[8,2048]{1,0:T(8,128)(2,1)S(1)}, u32[]{:S(2)}, u32[]{:S(2)}) collective-permute-start(bf16[8,2048]{1,0:T(8,128)(2,1)S(1)} %collective-permute-done.8), channel_id=1, source_target_pairs={{0,2},{2,4},{4,6},{6,8},{8,10},{10,12},{12,14},{14,16},{16,18},{18... | collective-permute-start | bytes 98312 | tf_op jit(solution)/shard_map/ppermute | solution.py:17
  138.5 0.6 copy-start.12
  139.1 7.5 %collective-permute-start.10 = (bf16[8,2048]{1,0:T(8,128)(2,1)S(1)}, bf16[8,2048]{1,0:T(8,128)(2,1)S(1)}, u32[]{:S(2)}, u32[]{:S(2)}) collective-permute-start(bf16[8,2048]{1,0:T(8,128)(2,1)S(1)} %collective-permute-done.9), channel_id=1, source_target_pairs={{0,2},{2,4},{4,6},{6,8},{8,10},{10,12},{12,14},{14,16},{16,18},{18... | collective-permute-start | bytes 98312 | tf_op jit(solution)/shard_map/ppermute | solution.py:17
  146.6 30.1 %copy-start.13 = (bf16[8,2048]{1,0:T(8,128)(2,1)}, bf16[8,2048]{1,0:T(8,128)(2,1)S(1)}, u32[]{:S(2)}) copy-start(bf16[8,2048]{1,0:T(8,128)(2,1)S(1)} %collective-permute-done.10) | copy-start | bytes 98308
  146.6 7.5 %collective-permute-start.11 = (bf16[8,2048]{1,0:T(8,128)(2,1)S(1)}, bf16[8,2048]{1,0:T(8,128)(2,1)S(1)}, u32[]{:S(2)}, u32[]{:S(2)}) collective-permute-start(bf16[8,2048]{1,0:T(8,128)(2,1)S(1)} %collective-permute-done.10), channel_id=1, source_target_pairs={{0,2},{2,4},{4,6},{6,8},{8,10},{10,12},{12,14},{14,16},{16,18},{18... | collective-permute-start | bytes 98312 | tf_op jit(solution)/shard_map/ppermute | solution.py:17
  154.1 22.6 %copy-start.14 = (bf16[8,2048]{1,0:T(8,128)(2,1)}, bf16[8,2048]{1,0:T(8,128)(2,1)S(1)}, u32[]{:S(2)}) copy-start(bf16[8,2048]{1,0:T(8,128)(2,1)S(1)} %collective-permute-done.11) | copy-start | bytes 98308
  154.1 7.5 %collective-permute-start.12 = (bf16[8,2048]{1,0:T(8,128)(2,1)S(1)}, bf16[8,2048]{1,0:T(8,128)(2,1)S(1)}, u32[]{:S(2)}, u32[]{:S(2)}) collective-permute-start(bf16[8,2048]{1,0:T(8,128)(2,1)S(1)} %collective-permute-done.11), channel_id=1, source_target_pairs={{0,2},{2,4},{4,6},{6,8},{8,10},{10,12},{12,14},{14,16},{16,18},{18... | collective-permute-start | bytes 98312 | tf_op jit(solution)/shard_map/ppermute | solution.py:17
  161.6 15.1 %copy-start.15 = (bf16[8,2048]{1,0:T(8,128)(2,1)}, bf16[8,2048]{1,0:T(8,128)(2,1)S(1)}, u32[]{:S(2)}) copy-start(bf16[8,2048]{1,0:T(8,128)(2,1)S(1)} %collective-permute-done.12) | copy-start | bytes 98308
  161.6 7.5 %collective-permute-start.13 = (bf16[8,2048]{1,0:T(8,128)(2,1)S(1)}, bf16[8,2048]{1,0:T(8,128)(2,1)S(1)}, u32[]{:S(2)}, u32[]{:S(2)}) collective-permute-start(bf16[8,2048]{1,0:T(8,128)(2,1)S(1)} %collective-permute-done.12), channel_id=1, source_target_pairs={{0,2},{2,4},{4,6},{6,8},{8,10},{10,12},{12,14},{14,16},{16,18},{18... | collective-permute-start | bytes 98312 | tf_op jit(solution)/shard_map/ppermute | solution.py:17
  169.1 7.6 %copy-start.16 = (bf16[8,2048]{1,0:T(8,128)(2,1)}, bf16[8,2048]{1,0:T(8,128)(2,1)S(1)}, u32[]{:S(2)}) copy-start(bf16[8,2048]{1,0:T(8,128)(2,1)S(1)} %collective-permute-done.13) | copy-start | bytes 98308
  169.1 7.6 %collective-permute-start.14 = (bf16[8,2048]{1,0:T(8,128)(2,1)S(1)}, bf16[8,2048]{1,0:T(8,128)(2,1)}, u32[]{:S(2)}, u32[]{:S(2)}) collective-permute-start(bf16[8,2048]{1,0:T(8,128)(2,1)S(1)} %collective-permute-done.13), channel_id=1, source_target_pairs={{0,2},{2,4},{4,6},{6,8},{8,10},{10,12},{12,14},{14,16},{16,18},{18... | collective-permute-start | bytes 98312 | tf_op jit(solution)/shard_map/ppermute | solution.py:17
  170.5 36.9 %all-to-all-start = ((bf16[32,3,2048]{2,1,0:T(4,128)(2,1)}), bf16[32,3,2048]{2,1,0:T(4,128)(2,1)S(1)}, u32[]{:S(2)}, u32[]{:S(2)}) async-start(bf16[32,3,2048]{2,1,0:T(4,128)(2,1)} %bitcast.11), calls=%async_computation.1 | async-start | bytes 1048576 | tf_op jit(solution)/shard_map/all_to_all | solution.py:140
  176.5 111.2 %reduce-scatter.5.cloned.1.call-start = ((), (), s32[]{:S(2)}) async-start(), calls=%async_computation.5 | async-start | bytes 1114112 | tf_op jit(solution)/shard_map/reduce_scatter | solution.py:126
  212.1 14.8 %copy-start.27 = (bf16[8,2]{0,1:T(2,128)(2,1)S(1)}, bf16[8,2]{0,1:T(2,128)(2,1)}, u32[]{:S(2)}) copy-start(bf16[8,2]{0,1:T(2,128)(2,1)} %param.39) | copy-start | bytes 100
  212.1 14.8 %copy-start.24 = (s32[8,2]{0,1:T(2,128)S(1)}, s32[8,2]{0,1:T(2,128)}, u32[]{:S(2)}) copy-start(s32[8,2]{0,1:T(2,128)} %param.38) | copy-start | bytes 196
  212.1 14.9 %copy-start.17 = (f32[2048]{0:T(1024)S(1)}, f32[2048]{0:T(1024)}, u32[]{:S(2)}) copy-start(f32[2048]{0:T(1024)} %param.21) | copy-start | bytes 24580
  212.2 14.9 %copy-start.21 = (f32[16]{0:T(128)S(1)}, f32[16]{0:T(128)}, u32[]{:S(2)}) copy-start(f32[16]{0:T(128)} %copy-done.20) | copy-start | bytes 196
  221.0 23.3 %all-to-all-start.1 = ((bf16[32,3,2048]{2,1,0:T(4,128)(2,1)}), bf16[32,3,2048]{2,1,0:T(4,128)(2,1)S(1)}, u32[]{:S(2)}, u32[]{:S(2)}) async-start(bf16[32,3,2048]{2,1,0:T(4,128)(2,1)} %convert_element_type.98), calls=%async_computation.2 | async-start | bytes 1048576 | tf_op jit(solution)/shard_map/all_to_all | solution.py:149
Sparse Core Ops, SparseCore 0:
  46.7 10.2 reduce-scatter.2
  207.5 80.1 reduce-scatter.4
